TPU v7x, 32 devices: a whole 2x2x4 slice. The times are simulated.
32 devices in a mesh: sp: 8 (over z, x), dp: 4 (over y, core).
Axes of the slice: x: 2, y: 2, z: 4, core: 2. Of those that a mesh axis runs over, the one named last changes fastest.
Arguments:
- residual: bfloat16 [4, 1024, 2048], P('dp', 'sp'), may hold values from -6 to 6
- query: bfloat16 [4, 1024, 2048], P('dp', 'sp'), may hold values from -6 to 6
- key: bfloat16 [4, 1024, 2048], P('dp', 'sp'), may hold values from -6 to 6
- value: bfloat16 [4, 1024, 2048], P('dp', 'sp'), may hold values from -6 to 6
- output_gate_input: bfloat16 [4, 1024, 2048], P('dp', 'sp'), may hold values from -6 to 6
- write_strength_logit: bfloat16 [4, 1024, 16], P('dp', 'sp'), may hold values from -6 to 6
- decay_head_input: bfloat16 [4, 1024, 16], P('dp', 'sp'), may hold values from -5 to 5
- added_log_decay: float32 [4, 16, 1024], P('dp', 'sp'), may hold values from -2 to 0
- head_decay_rate: float32 [16], P('sp'), may hold values from 0 to 1
- head_norm_gain: float32 [128], replicated, may hold values from 0.1 to 1.9
- output_projection: bfloat16 [2048, 2048], P(None, 'dp'), may hold values from -0.125 to 0.125
- mixer_norm_gain: float32 [2048], replicated, may hold values from 0.1 to 1.9
- token_expert_index: int32 [4, 1024, 4], P('dp', 'sp'), may hold values from 0 to 31, all different within a row; in each aligned block of 128 rows (0 to 127, 128 to 255, ..., all dimensions but the last counted through in order) at most 24 rows name the same one
- token_expert_weight: float32 [4, 1024, 4], P('dp', 'sp'), may hold values from 0.1 to 0.6
- expert_gate_weight: bfloat16 [32, 2048, 1024], P(('sp', 'dp')), may hold values from -1 to 1
- expert_up_weight: bfloat16 [32, 2048, 1024], P(('sp', 'dp')), may hold values from -1 to 1
- expert_down_weight: bfloat16 [32, 1024, 2048], P(('sp', 'dp')), may hold values from -0.1875 to 0.1875
- feedforward_norm_gain: float32 [2048], replicated, may hold values from 0.1 to 1.9
Outputs:
- blended: float32 [4, 1024, 2048], P('dp', 'sp')
Inputs may be any that keep to these rules, and one draw needn't show every extreme that they name: `token_expert_index`: each row names 4 different experts; within the 128 rows of one device no expert is named by more than 24 rows, and in every draw some expert is named by exactly 24 rows of some device.
All inputs are finite; a program needn't handle non-finite values.
Results may differ from a plain program's by a relative error of at most 0.0062.
Values may be sent and summed in bfloat16 or wider, within the bound.
A program may use at most 128 MiB of HBM per device.

v0:
```python
import functools

import jax
import jax.numpy as jnp
from jax import lax
from jax.experimental import pallas as pl
from jax.experimental.pallas import tpu as pltpu
from jax.sharding import PartitionSpec as P

CLAMP_LIMIT = 7.0
SWISH_SLOPE = 1.702
MESH = pl.DeviceIdType.MESH


def greet_peers(count):
    me = lax.axis_index("sp")
    barrier = pltpu.get_barrier_semaphore()
    for offset in range(1, count):
        pl.semaphore_signal(
            barrier, inc=1, device_id={"sp": lax.rem(me + offset, count)}, device_id_type=MESH
        )
    pl.semaphore_wait(barrier, count - 1)


def spread_heads_kernel(count, *refs):
    arrays = (len(refs) - 3) // 2
    sources, targets = refs[:arrays], refs[arrays : 2 * arrays]
    send_sem, recv_sem, local_sem = refs[2 * arrays :]
    me = lax.axis_index("sp")

    def piece(source, owner):
        if source.shape[0] == count:
            return source.at[owner]
        width = source.shape[2] // count
        return source.at[0, :, pl.ds(pl.multiple_of(owner * width, width), width)]

    def place(target, owner):
        return target.at[owner]

    greet_peers(count)
    copies = []
    for offset in range(1, count):
        peer = lax.rem(me + offset, count)
        for at in range(arrays):
            copy = pltpu.make_async_remote_copy(
                src_ref=piece(sources[at], peer),
                dst_ref=place(targets[at], me),
                send_sem=send_sem.at[at, offset],
                recv_sem=recv_sem.at[at, offset],
                device_id={"sp": peer},
                device_id_type=MESH,
            )
            copy.start()
            copies.append(copy)
    for at in range(arrays):
        copy = pltpu.make_async_copy(
            piece(sources[at], me), place(targets[at], me), local_sem.at[at]
        )
        copy.start()
        copies.append(copy)
    for copy in copies:
        copy.wait()


def spread_heads(sources, count):
    shapes = []
    for source in sources:
        if source.shape[0] == count:
            shapes.append(jax.ShapeDtypeStruct(source.shape, source.dtype))
        else:
            shapes.append(
                jax.ShapeDtypeStruct(
                    (count, source.shape[1], source.shape[2] // count), source.dtype
                )
            )
    return pl.pallas_call(
        functools.partial(spread_heads_kernel, count),
        out_shape=shapes,
        in_specs=[pl.BlockSpec(memory_space=pltpu.VMEM)] * len(sources),
        out_specs=[pl.BlockSpec(memory_space=pl.ANY)] * len(sources),
        scratch_shapes=[
            pltpu.SemaphoreType.DMA((len(sources), count)),
            pltpu.SemaphoreType.DMA((len(sources), count)),
            pltpu.SemaphoreType.DMA((len(sources),)),
        ],
        compiler_params=pltpu.CompilerParams(collective_id=0, has_side_effects=True),
    )(*sources)


def return_rows_kernel(count, source, target, send_sem, recv_sem, local_sem):
    me = lax.axis_index("sp")
    width = source.shape[2]
    own_columns = pl.ds(pl.multiple_of(me * width, width), width)
    greet_peers(count)
    copies = []
    for offset in range(1, count):
        peer = lax.rem(me + offset, count)
        copy = pltpu.make_async_remote_copy(
            src_ref=source.at[peer],
            dst_ref=target.at[:, own_columns],
            send_sem=send_sem.at[offset],
            recv_sem=recv_sem.at[offset],
            device_id={"sp": peer},
            device_id_type=MESH,
        )
        copy.start()
        copies.append(copy)
    copy = pltpu.make_async_copy(source.at[me], target.at[:, own_columns], local_sem)
    copy.start()
    copies.append(copy)
    for copy in copies:
        copy.wait()


def return_rows(source, count):
    return pl.pallas_call(
        functools.partial(return_rows_kernel, count),
        out_shape=jax.ShapeDtypeStruct(
            (source.shape[1], source.shape[2] * count), source.dtype
        ),
        in_specs=[pl.BlockSpec(memory_space=pltpu.VMEM)],
        out_specs=pl.BlockSpec(memory_space=pltpu.VMEM),
        scratch_shapes=[
            pltpu.SemaphoreType.DMA((count,)),
            pltpu.SemaphoreType.DMA((count,)),
            pltpu.SemaphoreType.DMA,
        ],
        compiler_params=pltpu.CompilerParams(collective_id=1, has_side_effects=True),
    )(source)


def dot(left, right):
    return jnp.dot(left, right, preferred_element_type=jnp.float32)


def halves(values):
    high = values.astype(jnp.bfloat16)
    return high, (values - high.astype(jnp.float32)).astype(jnp.bfloat16)


def dot3(left, right):
    return dot(left[0], right[0]) + (dot(left[0], right[1]) + dot(left[1], right[0]))


def rows_by_rows(left, right):
    return lax.dot_general(
        left, right, (((1,), (1,)), ((), ())), preferred_element_type=jnp.float32
    )


def recurrence_kernel(
    q_ref, k_ref, v_ref, small_ref, added_ref, decay_ref, gain_ref, out_ref,
    base_ref, weight_high, weight_low, score_ref, column_ref, state_ref,
):
    blocks, span, width = q_ref.shape
    heads = added_ref.shape[1]
    head_dim = width // heads
    row = lax.broadcasted_iota(jnp.int32, (span, span), 0)
    column = lax.broadcasted_iota(jnp.int32, (span, span), 1)
    same = row == column
    inclusive = row >= column
    strict = row > column
    identity = same.astype(jnp.float32)

    def to_column(values):
        return jnp.sum(jnp.where(same, values, 0.0), axis=1, keepdims=True)

    def to_row(values):
        return jnp.sum(jnp.where(same, values, 0.0), axis=0, keepdims=True)

    lanes = lax.broadcasted_iota(jnp.int32, (span, head_dim), 1)
    together = 2 if blocks % 2 == 0 else 1

    def prepare(step, carry):
        chains = [(step * together + i, h) for i in range(together) for h in range(heads)]
        lowers = []
        kept = []
        for block, head in chains:
            columns = slice(head * head_dim, (head + 1) * head_dim)
            q_raw = q_ref[block, :, columns]
            k_raw = k_ref[block, :, columns]
            q_wide = q_raw.astype(jnp.float32)
            q_rate = (
                lax.rsqrt(jnp.sum(q_wide * q_wide, 1, keepdims=True) + 1e-06)
                * head_dim ** (-0.5)
            )
            k_dot = rows_by_rows(k_raw, k_raw)
            k_wide = k_raw.astype(jnp.float32)
            k_rate = lax.rsqrt(jnp.sum(k_wide * k_wide, 1, keepdims=True) + 1e-06)
            k_rate_row = to_row(k_rate)
            rate_row = jax.nn.sigmoid(small_ref[block, head : head + 1, :])
            sequence_row = small_ref[block, heads + head : heads + head + 1, :]
            softplus = jnp.maximum(sequence_row, 0.0) + jnp.log1p(
                jnp.exp(-jnp.abs(sequence_row))
            )
            log_decay = (
                added_ref[block, head : head + 1, :] - decay_ref[head] * softplus
            )
            total = jnp.sum(jnp.where(inclusive, log_decay, 0.0), axis=1, keepdims=True)
            total_row = to_row(total)
            last = total[span - 1 : span, :]
            within = jnp.exp(jnp.where(inclusive, total - total_row, -1e30))
            lower = jnp.where(
                strict, to_column(rate_row) * within * k_dot * (k_rate * k_rate_row), 0.0
            )
            scores = rows_by_rows(q_raw, k_raw) * within * (q_rate * k_rate_row)
            rows = pl.ds(pl.multiple_of(block * span, span), span)
            score_ref[head, rows, :] = scores.astype(jnp.bfloat16)
            column_ref[head, rows, :] = jnp.where(
                lanes == 0,
                q_rate * jnp.exp(total),
                jnp.where(lanes == 1, k_rate * jnp.exp(last - total), jnp.exp(last)),
            )
            lowers.append(lower)
            kept.append((rate_row, rate_row * jnp.exp(total_row) * k_rate_row))
        inverses = [
            identity - jnp.where((row // 2) == (column // 2), lower, 0.0) for lower in lowers
        ]
        size = 2
        while size < span:
            joined = ((row // (2 * size)) == (column // (2 * size))) & (
                (row // size) != (column // size)
            )
            parts = [halves(inverse) for inverse in inverses]
            corner = [halves(jnp.where(joined, lower, 0.0)) for lower in lowers]
            first = [halves(dot3(p, c)) for p, c in zip(parts, corner)]
            inverses = [
                inverse - dot3(f, p) for inverse, f, p in zip(inverses, first, parts)
            ]
            size *= 2
        for (block, head), inverse, (value_rate, key_rate) in zip(chains, inverses, kept):
            columns = slice(head * head_dim, (head + 1) * head_dim)
            rows = pl.ds(pl.multiple_of(block * span, span), span)
            high, low = halves(inverse * value_rate)
            v_raw = v_ref[block, :, columns]
            base_ref[head, rows, :] = dot(high, v_raw) + dot(low, v_raw)
            high, low = halves(inverse * key_rate)
            k_raw = k_ref[block, :, columns]
            weight = halves(dot(high, k_raw) + dot(low, k_raw))
            weight_high[head, rows, :] = weight[0]
            weight_low[head, rows, :] = weight[1]
        return carry

    lax.fori_loop(0, blocks // together, prepare, 0)
    state_ref[...] = jnp.zeros_like(state_ref)
    gain = gain_ref[...]

    def advance(block, carry):
        rows = pl.ds(pl.multiple_of(block * span, span), span)
        for head in range(heads):
            columns = slice(head * head_dim, (head + 1) * head_dim)
            state = state_ref[head]
            parts = halves(state)
            scales = column_ref[head, rows, :]
            fresh = base_ref[head, rows, :] - dot3(
                (weight_high[head, rows, :], weight_low[head, rows, :]), parts
            )
            moved = halves(fresh * scales[:, 1:2])
            k_raw = k_ref[block, :, columns]
            q_raw = q_ref[block, :, columns]
            turned = (((0,), (0,)), ((), ()))
            gained = lax.dot_general(
                k_raw, moved[0], turned, preferred_element_type=jnp.float32
            ) + lax.dot_general(k_raw, moved[1], turned, preferred_element_type=jnp.float32)
            state_ref[head] = state * scales[:, 2:3] + gained
            output = (dot(q_raw, parts[0]) + dot(q_raw, parts[1])) * scales[:, 0:1] + dot(
                score_ref[head, rows, :], fresh.astype(jnp.bfloat16)
            )
            norm_scale = lax.rsqrt(jnp.mean(output * output, -1, keepdims=True) + 1e-05)
            out_ref[block, :, columns] = (output * norm_scale * gain).astype(jnp.bfloat16)
        return carry

    lax.fori_loop(0, blocks, advance, 0)


def recurrence(q_blocks, k_blocks, v_blocks, small, added, head_decay_rate, head_norm_gain):
    blocks, span, width = q_blocks.shape
    heads = head_decay_rate.shape[0]
    head_dim = width // heads
    vmem = pl.BlockSpec(memory_space=pltpu.VMEM)
    length = blocks * span
    return pl.pallas_call(
        recurrence_kernel,
        out_shape=jax.ShapeDtypeStruct(q_blocks.shape, jnp.bfloat16),
        in_specs=[vmem] * 5 + [pl.BlockSpec(memory_space=pltpu.SMEM), vmem],
        out_specs=vmem,
        scratch_shapes=[
            pltpu.VMEM((heads, length, head_dim), jnp.float32),
            pltpu.VMEM((heads, length, head_dim), jnp.bfloat16),
            pltpu.VMEM((heads, length, head_dim), jnp.bfloat16),
            pltpu.VMEM((heads, length, span), jnp.bfloat16),
            pltpu.VMEM((heads, length, head_dim), jnp.float32),
            pltpu.VMEM((heads, head_dim, head_dim), jnp.float32),
        ],
        cost_estimate=pl.CostEstimate(
            flops=heads * blocks * 40 * 2 * span * span * head_dim * 16,
            bytes_accessed=4 * length * width * 2,
            transcendentals=0,
        ),
    )(q_blocks, k_blocks, v_blocks, small, added, head_decay_rate, head_norm_gain[None, :])


def projection_pieces(weight):
    count = lax.axis_size("dp")
    pair = [(at, at ^ 1) for at in range(count)]
    me = lax.axis_index("dp")
    pieces = []
    for shift in range(0, count, 2):
        if shift == 0:
            moved = weight
        else:
            moved = lax.ppermute(
                weight, "dp", [(at, (at + shift) % count) for at in range(count)]
            )
        pieces.append((lax.rem(me - shift + count, count), moved))
        other = me + 1 - 2 * lax.rem(me, 2)
        pieces.append((lax.rem(other - shift + count, count), lax.ppermute(moved, "dp", pair)))
    return pieces


def layer_norm(values, gain):
    average = jnp.mean(values, -1, keepdims=True)
    centred = values - average
    variance = jnp.mean(centred * centred, -1, keepdims=True)
    return centred * lax.rsqrt(variance + 1e-05) * gain


def expert_rows(rows, gate_weight, up_weight, down_weight):
    flat_rows = rows.reshape(-1, rows.shape[-1])
    gate = jnp.minimum(
        jnp.dot(flat_rows, gate_weight, preferred_element_type=jnp.float32), CLAMP_LIMIT
    )
    upper = jnp.clip(
        jnp.dot(flat_rows, up_weight, preferred_element_type=jnp.float32), -CLAMP_LIMIT, CLAMP_LIMIT
    )
    hidden = (gate * jax.nn.sigmoid(SWISH_SLOPE * gate) * (upper + 1.0)).astype(jnp.bfloat16)
    produced = jnp.dot(hidden, down_weight, preferred_element_type=jnp.float32).astype(jnp.bfloat16)
    return produced.reshape(rows.shape)


def per_device(
    residual,
    query,
    key,
    value,
    output_gate_input,
    write_strength_logit,
    decay_head_input,
    added_log_decay,
    head_decay_rate,
    head_norm_gain,
    output_projection,
    mixer_norm_gain,
    token_expert_index,
    token_expert_weight,
    expert_gate_weight,
    expert_up_weight,
    expert_down_weight,
    feedforward_norm_gain,
):
    count = lax.axis_size("sp")
    tokens = query.shape[1]
    local_heads = head_decay_rate.shape[0]
    pieces = projection_pieces(output_projection)
    small = jnp.concatenate(
        [
            write_strength_logit[0].T.reshape(count, local_heads, tokens),
            decay_head_input[0].T.reshape(count, local_heads, tokens),
            jnp.zeros((count, 8 - 2 * local_heads, tokens), jnp.bfloat16),
        ],
        axis=1,
    ).astype(jnp.float32)
    q_blocks, k_blocks, v_blocks, small_blocks = spread_heads(
        (query, key, value, small), count
    )
    added = added_log_decay[0].reshape(local_heads, count, tokens).transpose(1, 0, 2)
    scaled = recurrence(
        q_blocks, k_blocks, v_blocks, small_blocks, added, head_decay_rate, head_norm_gain
    )
    returned = return_rows(scaled, count)
    token_rows = (
        returned.astype(jnp.float32) * jax.nn.silu(output_gate_input[0].astype(jnp.float32))
    ).astype(jnp.bfloat16)
    width = output_projection.shape[1]
    mixed = jnp.zeros((tokens, width * len(pieces)), jnp.float32)
    for owner, piece in pieces:
        mixed = lax.dynamic_update_slice(
            mixed,
            jnp.dot(token_rows, piece, preferred_element_type=jnp.float32),
            (0, owner * width),
        )
    normed = layer_norm(residual[0].astype(jnp.float32) + mixed, mixer_norm_gain).astype(
        jnp.bfloat16
    )
    experts = lax.axis_size("sp") * lax.axis_size("dp")
    tok_rows = normed.shape[0]
    picks = token_expert_index.shape[2]
    features = normed.shape[1]
    capacity = tok_rows * picks * 3 // (2 * experts)
    flat_ids = token_expert_index[0].reshape(-1)
    onehot = (flat_ids[:, None] == jnp.arange(experts, dtype=jnp.int32)[None, :]).astype(jnp.int32)
    earlier = jnp.cumsum(onehot, axis=0) - onehot
    slot_rank = jnp.sum(earlier * onehot, axis=1)
    destination = flat_ids * capacity + slot_rank
    source_token = (
        jnp.full((experts * capacity,), tok_rows, jnp.int32)
        .at[destination]
        .set(jnp.arange(tok_rows * picks, dtype=jnp.int32) // picks)
    )
    padded = jnp.concatenate([normed, jnp.zeros((1, features), jnp.bfloat16)], 0)
    dispatch = padded[source_token].reshape(experts, capacity, features)
    back = lax.all_to_all(
        expert_rows(
            lax.all_to_all(dispatch, ("sp", "dp"), split_axis=0, concat_axis=0, tiled=True),
            expert_gate_weight[0],
            expert_up_weight[0],
            expert_down_weight[0],
        ),
        ("sp", "dp"),
        split_axis=0,
        concat_axis=0,
        tiled=True,
    )
    results = back.reshape(experts * capacity, features)[destination].reshape(
        tok_rows, picks, features
    )
    weights = token_expert_weight[0]
    moe = jnp.zeros((tok_rows, features), jnp.float32)
    for pick in range(picks):
        moe = moe + weights[:, pick : pick + 1] * results[:, pick].astype(jnp.float32)
    return layer_norm(normed.astype(jnp.float32) + moe, feedforward_norm_gain)[None]


def solution(mesh):
    placed = (
        P("dp", "sp", None),
        P("dp", "sp", None),
        P("dp", "sp", None),
        P("dp", "sp", None),
        P("dp", "sp", None),
        P("dp", "sp", None),
        P("dp", "sp", None),
        P("dp", "sp", None),
        P("sp"),
        P(),
        P(None, "dp"),
        P(),
        P("dp", "sp", None),
        P("dp", "sp", None),
        P(("sp", "dp"), None, None),
        P(("sp", "dp"), None, None),
        P(("sp", "dp"), None, None),
        P(),
    )
    return jax.shard_map(
        per_device, mesh=mesh, in_specs=placed, out_specs=P("dp", "sp", None), check_vma=False
    )
```

profile of v0, /device:TPU:0, one launch (start us, length us, event | category | flops | bytes accessed | tf_op | source)
XLA Modules:
  0.0 277.0 jit_solution(17592283697823687325)
XLA Ops:
  0.5 2.5 collective-permute-start.1
  3.1 1.4 maximum_convert_fusion.refs_3_
  4.5 32.7 %shard_map.172 = (bf16[8,128,256]{2,1,0:T(8,128)(2,1)}, bf16[8,128,256]{2,1,0:T(8,128)(2,1)}, bf16[8,128,256]{2,1,0:T(8,128)(2,1)}, f32[8,8,128]{2,1,0:T(8,128)}) custom-call(bf16[1,128,2048]{2,1,0:T(8,128)(2,1)} %refs_0_.1, bf16[1,128,2048]{2,1,0:T(8,128)(2,1)} %refs_1_.1, bf16[1,128,2048]{2,1,0:T(8,128)(2,1)} %refs_2_.1, ...), custom_call_target="tpu_custom_call" | custom-call | tf_op jit(solution)/shard_map/pallas_call | solution.py:76
  37.2 18.4 %shard_map.173.source = bf16[8,128,256]{2,1,0:T(8,128)(2,1)} custom-call(bf16[8,128,256]{2,1,0:T(8,128)(2,1)} %get-tuple-element.9.q_ref, bf16[8,128,256]{2,1,0:T(8,128)(2,1)} %get-tuple-element.10.k_ref, bf16[8,128,256]{2,1,0:T(8,128)(2,1)} %get-tuple-element.11.v_ref, f32[8,8,128]{2,1,0:T(8,128)} %get-tuple-element.12.small_ref, f32[8,2,128]{2,1,0:T(2,128)} %bitcast.121, ...), custom_call_target="tpu_custom_call" | custom-call | flops 42949672960 | bytes 2097152 | tf_op jit(solution)/shard_map/pallas_call | solution.py:282
  55.8 1.2 reduce-window.6
  57.5 24.0 %shard_map.174 = bf16[128,2048]{1,0:T(8,128)(2,1)} custom-call(bf16[8,128,256]{2,1,0:T(8,128)(2,1)} %shard_map.173.source), custom_call_target="tpu_custom_call" | custom-call | tf_op jit(solution)/shard_map/pallas_call | solution.py:116
  81.9 2.4 scatter_custom_fusion
  84.4 1.4 fusion.19
  86.4 2.0 convolution_dynamic-update-slice_fusion.2
  88.4 2.1 convolution_dynamic-update-slice_fusion.1
  90.5 2.0 convolution_dynamic-update-slice_fusion
  93.4 0.8 copy-done.1
  94.2 4.3 %gather_fusion = bf16[768,2048]{1,0:T(8,128)(2,1)} fusion(bf16[129,2048]{1,0:T(8,128)(2,1)S(1)} %concatenate.7, s32[1024]{0:T(1024)S(1)} %pad_clamp_fusion.1), kind=kCustom, calls=%fused_computation | custom fusion | bytes 6294528 | tf_op jit(solution)/shard_map/gather | solution.py:411
  98.5 78.6 %all_to_all.10 = bf16[32,24,2048]{2,1,0:T(8,128)(2,1)S(1)} all-to-all(bf16[32,24,2048]{2,1,0:T(8,128)(2,1)} %bitcast.111), channel_id=1, replica_groups=mesh['sp'=8,'dp'=4] {'sp','dp'}, dimensions={0} | all-to-all | bytes 6291456 | tf_op jit(solution)/shard_map/all_to_all | solution.py:414
  177.0 3.4 %fusion.2 = f32[768,1024]{1,0:T(8,128)S(1)} fusion(bf16[768,2048]{1,0:T(8,128)(2,1)S(1)} %bitcast.113, bf16[1,2048,1024]{2,1,0:T(8,128)(2,1)S(1)} %copy-done.9), kind=kOutput, calls=%fused_computation.5 | convolution fusion | flops 3221225472 | bytes 10485760 | tf_op jit(solution)/shard_map/dot_general | solution.py:334
  180.5 4.1 %multiply_convert_fusion = bf16[768,1024]{1,0:T(8,128)(2,1)S(1)} fusion(f32[768,1024]{1,0:T(8,128)S(1)} %fusion.2, bf16[768,2048]{1,0:T(8,128)(2,1)S(1)} %bitcast.114, bf16[1,2048,1024]{2,1,0:T(8,128)(2,1)S(1)} %copy-done.10), kind=kOutput, calls=%fused_computation.10 | convolution fusion | flops 3229089792 | bytes 12058624 | tf_op jit(solution)/shard_map/dot_general | solution.py:331
  184.7 4.8 %fusion.6 = bf16[768,2048]{1,0:T(8,128)(2,1)} fusion(bf16[768,1024]{1,0:T(8,128)(2,1)S(1)} %multiply_convert_fusion, bf16[1,1024,2048]{2,1,0:T(8,128)(2,1)S(1)} %copy-done.11), kind=kOutput, calls=%fused_computation.9 | convolution fusion | flops 3222798336 | bytes 8912896 | tf_op jit(solution)/shard_map/dot_general | solution.py:337
  189.5 3.7 %all-to-all-start.1 = ((bf16[32,24,2048]{2,1,0:T(8,128)(2,1)}), bf16[32,24,2048]{2,1,0:T(8,128)(2,1)S(1)}, u32[]{:S(2)}, u32[]{:S(2)}) async-start(bf16[32,24,2048]{2,1,0:T(8,128)(2,1)} %bitcast.112), calls=%async_computation.1 | async-start | bytes 6291456 | tf_op jit(solution)/shard_map/all_to_all | solution.py:412
  193.2 71.6 %all-to-all-done.1 = bf16[32,24,2048]{2,1,0:T(8,128)(2,1)S(1)} async-done(((bf16[32,24,2048]{2,1,0:T(8,128)(2,1)}), bf16[32,24,2048]{2,1,0:T(8,128)(2,1)S(1)}, u32[]{:S(2)}, u32[]{:S(2)}) %all-to-all-start.1) | async-done | bytes 3145760 | tf_op jit(solution)/shard_map/all_to_all | solution.py:412
  264.8 3.3 %gather_fusion.1 = bf16[512,2048]{1,0:T(8,128)(2,1)} fusion(bf16[768,2048]{1,0:T(8,128)(2,1)S(1)} %bitcast.110, s32[1024]{0:T(1024)S(1)} %pad_clamp_fusion), kind=kCustom, calls=%fused_computation.1 | custom fusion | bytes 4196352 | tf_op jit(solution)/shard_map/gather | solution.py:424
  268.1 2.7 reshape.111
  270.9 3.1 %fusion.32 = (bf16[128,1,2048]{2,1,0:T(2,128)(2,1)S(1)}, bf16[128,1,2048]{2,1,0:T(2,128)(2,1)S(1)}, bf16[128,1,2048]{2,1,0:T(2,128)(2,1)S(1)}, bf16[128,1,2048]{2,1,0:T(2,128)(2,1)S(1)}) fusion(bf16[128,4,2048]{2,1,0:T(4,128)(2,1)S(1)} %reshape.111), kind=kLoop, calls=%fused_computation.73 | loop fusion | bytes 4194304 | tf_op jit(solution)/shard_map/slice | solution.py:430
  274.0 1.6 fusion.30
  275.9 1.2 multiply_bitcast_fusion
  (58 shorter events, 3.3 us)
Async XLA Ops:
  0.0 86.3 %collective-permute-start = (bf16[2048,512]{1,0:T(8,128)(2,1)}, bf16[2048,512]{1,0:T(8,128)(2,1)}, u32[]{:S(2)}, u32[]{:S(2)}) collective-permute-start(bf16[2048,512]{1,0:T(8,128)(2,1)} %param.28), channel_id=1, source_target_pairs={{0,1},{1,0},{2,3},{3,2},{4,5},{5,4},{6,7},{7,6},{8,9},{9,8},{10,11... | collective-permute-start | bytes 6291464 | tf_op jit(solution)/shard_map/ppermute | solution.py:317
  0.5 56.8 %collective-permute-start.1 = (bf16[2048,512]{1,0:T(8,128)(2,1)}, bf16[2048,512]{1,0:T(8,128)(2,1)}, u32[]{:S(2)}, u32[]{:S(2)}) collective-permute-start(bf16[2048,512]{1,0:T(8,128)(2,1)} %param.28), channel_id=1, source_target_pairs={{0,2},{1,3},{2,0},{3,1},{4,6},{5,7},{6,4},{7,5},{8,10},{9,11},{10,... | collective-permute-start | bytes 6291464 | tf_op jit(solution)/shard_map/ppermute | solution.py:312
  37.2 18.4 %copy-start.7 = (s32[1,128,4]{1,2,0:T(4,128)S(1)}, s32[1,128,4]{1,2,0:T(4,128)}, u32[]{:S(2)}) copy-start(s32[1,128,4]{1,2,0:T(4,128)} %param.30) | copy-start | bytes 6148
  37.2 47.2 %copy-start.4 = (bf16[1,128,2048]{2,1,0:T(8,128)(2,1)S(1)}, bf16[1,128,2048]{2,1,0:T(8,128)(2,1)}, u32[]{:S(2)}) copy-start(bf16[1,128,2048]{2,1,0:T(8,128)(2,1)} %param.22) | copy-start | bytes 1572868
  55.6 30.3 %copy-start.3 = (bf16[2048,512]{1,0:T(8,128)(2,1)S(1)}, bf16[2048,512]{1,0:T(8,128)(2,1)}, u32[]{:S(2)}) copy-start(bf16[2048,512]{1,0:T(8,128)(2,1)} %param.28) | copy-start | bytes 6291460
  57.3 33.3 %collective-permute-start.2 = (bf16[2048,512]{1,0:T(8,128)(2,1)}, bf16[2048,512]{1,0:T(8,128)(2,1)}, u32[]{:S(2)}, u32[]{:S(2)}) collective-permute-start(bf16[2048,512]{1,0:T(8,128)(2,1)} %collective-permute-done.1), channel_id=1, source_target_pairs={{0,1},{1,0},{2,3},{3,2},{4,5},{5,4},{6,7},{7,6},{8,9},{9,8},{10,11... | collective-permute-start | bytes 6291464 | tf_op jit(solution)/shard_map/ppermute | solution.py:317
  88.4 4.2 %copy-start = (bf16[1,128,2048]{2,1,0:T(8,128)(2,1)S(1)}, bf16[1,128,2048]{2,1,0:T(8,128)(2,1)}, u32[]{:S(2)}) copy-start(bf16[1,128,2048]{2,1,0:T(8,128)(2,1)} %param.18) | copy-start | bytes 1572868
  90.5 2.6 copy-start.5
  93.4 0.8 copy-start.1
  98.5 78.6 %copy-start.9 = (bf16[1,2048,1024]{2,1,0:T(8,128)(2,1)S(1)}, bf16[1,2048,1024]{2,1,0:T(8,128)(2,1)}, u32[]{:S(2)}) copy-start(bf16[1,2048,1024]{2,1,0:T(8,128)(2,1)} %param.33) | copy-start | bytes 12582916
  177.0 3.5 %copy-start.10 = (bf16[1,2048,1024]{2,1,0:T(8,128)(2,1)S(1)}, bf16[1,2048,1024]{2,1,0:T(8,128)(2,1)}, u32[]{:S(2)}) copy-start(bf16[1,2048,1024]{2,1,0:T(8,128)(2,1)} %param.32) | copy-start | bytes 12582916
  180.5 4.2 %copy-start.11 = (bf16[1,1024,2048]{2,1,0:T(8,128)(2,1)S(1)}, bf16[1,1024,2048]{2,1,0:T(8,128)(2,1)}, u32[]{:S(2)}) copy-start(bf16[1,1024,2048]{2,1,0:T(8,128)(2,1)} %param.34) | copy-start | bytes 12582916
  189.5 3.7 %copy-start.8 = (f32[1,128,4]{1,2,0:T(4,128)S(1)}, f32[1,128,4]{1,2,0:T(4,128)}, u32[]{:S(2)}) copy-start(f32[1,128,4]{1,2,0:T(4,128)} %param.31) | copy-start | bytes 6148
  189.5 75.3 %all-to-all-start.1 = ((bf16[32,24,2048]{2,1,0:T(8,128)(2,1)}), bf16[32,24,2048]{2,1,0:T(8,128)(2,1)S(1)}, u32[]{:S(2)}, u32[]{:S(2)}) async-start(bf16[32,24,2048]{2,1,0:T(8,128)(2,1)} %bitcast.112), calls=%async_computation.1 | async-start | bytes 6291456 | tf_op jit(solution)/shard_map/all_to_all | solution.py:412
  270.8 3.1 %copy-start.2 = (bf16[128,2048]{1,0:T(8,128)(2,1)S(1)}, bf16[128,2048]{1,0:T(8,128)(2,1)}, u32[]{:S(2)}) copy-start(bf16[128,2048]{1,0:T(8,128)(2,1)} %copy-done.1) | copy-start | bytes 1572868
  273.9 1.9 copy-start.6
where the time goes:
time: 278 us; the launch traced here: 277 us
  blocking collectives  78.6 us (28%)
  Pallas kernels  75.1 us (27%)
  waiting for transfers between devices  71.6 us (26%)
  matrix products  19 us (7%)
  local copies, waits for them, and re-layouts  17.7 us (6%)
  other arithmetic  7.91 us (3%)
  starting transfers between devices  6.73 us (2%)
    all_to_all x1, blocking collectives, per_device(): lax.all_to_all(dispatch, ('sp', 'dp'), split_axis=0, concat_axis=0, tiled...  78.6 us
    all_to_all x1, waiting for transfers between devices, per_device(): lax.all_to_all(expert_rows(lax.all_to_all(dispatch, ('sp', 'dp'), split_a...  71.6 us
    pallas_call x1, Pallas kernels, spread_heads(): pl.pallas_call(functools.partial(spread_heads_kernel, count), out_shape=s...  32.7 us
    pallas_call x1, Pallas kernels, return_rows(): pl.pallas_call(functools.partial(return_rows_kernel, count), out_shape=ja...  24 us
    pallas_call x1, Pallas kernels, recurrence(): pl.pallas_call(recurrence_kernel, out_shape=jax.ShapeDtypeStruct(q_blocks...  18.4 us
    dot_general x4, matrix products, per_device(): jnp.dot(token_rows, piece, preferred_element_type=jnp.float32)  6.62 us
  transfers between devices with their start and end apart: 4, of which 1 were waited for; matrix products, arithmetic and copies ran while one was open for 4% of the time, Pallas kernels for 27%

commit v1 on v0

--- a/solution.py
+++ b/solution.py
@@ -318,6 +318,379 @@
     return pieces
 
 
+def plane_split(count):
+    across = 1 << ((count.bit_length() - 1) // 2)
+    return count // across, across
+
+
+def dispatch_kernel(
+    layers, across, cores, rows_ref, pick_ref, out_ref, held, staged,
+    row_send, row_recv, out_send, out_recv, local_sem,
+):
+    experts = across * cores
+    place = lax.axis_index("sp")
+    core = lax.axis_index("dp")
+    layer = lax.div(place, across)
+    column = lax.rem(place, across)
+    member = column * cores + core
+    capacity = staged.shape[2]
+    features = rows_ref.shape[1]
+    tile = features // 4
+
+    def peer_at(offset):
+        other = lax.rem(member + offset, experts)
+        where = {"sp": layer * across + lax.div(other, cores), "dp": lax.rem(other, cores)}
+        return other, where
+
+    def row_copy(source, slot, way):
+        step = 1 - 2 * way
+        return pltpu.make_async_remote_copy(
+            src_ref=source,
+            dst_ref=held.at[slot],
+            send_sem=row_send.at[way, slot],
+            recv_sem=row_recv.at[slot],
+            device_id={"sp": lax.rem(place + step * across + layers * across, layers * across)},
+            device_id_type=MESH,
+        )
+
+    def out_copy(slot, offset):
+        other, where = peer_at(offset)
+        return pltpu.make_async_remote_copy(
+            src_ref=staged.at[slot, other],
+            dst_ref=out_ref.at[slot * experts + member],
+            send_sem=out_send.at[slot, offset],
+            recv_sem=out_recv.at[slot, offset],
+            device_id=where,
+            device_id_type=MESH,
+        )
+
+    def own_copy(slot):
+        return pltpu.make_async_copy(
+            staged.at[slot, member], out_ref.at[slot * experts + member], local_sem.at[slot]
+        )
+
+    barrier = pltpu.get_barrier_semaphore()
+    for offset in range(1, experts):
+        pl.semaphore_signal(
+            barrier, inc=1, device_id=peer_at(offset)[1], device_id_type=MESH
+        )
+
+    @pl.when(layer > 0)
+    def _():
+        pl.semaphore_signal(
+            barrier, inc=1, device_id={"sp": place - across}, device_id_type=MESH
+        )
+
+    @pl.when(layer < layers - 1)
+    def _():
+        pl.semaphore_signal(
+            barrier, inc=1, device_id={"sp": place + across}, device_id_type=MESH
+        )
+
+    inner = (layer > 0) & (layer < layers - 1)
+
+    @pl.when(inner)
+    def _():
+        pl.semaphore_wait(barrier, experts + 1)
+
+    @pl.when(jnp.logical_not(inner))
+    def _():
+        pl.semaphore_wait(barrier, experts if layers > 1 else experts - 1)
+
+    def serve(slot, source):
+        picks = pick_ref[slot]
+        for at in range(4):
+            columns = slice(at * tile, (at + 1) * tile)
+            chosen = jnp.dot(picks, source[:, columns], preferred_element_type=jnp.float32)
+            staged[slot, :, :, columns] = chosen.reshape(experts, capacity, tile).astype(
+                jnp.bfloat16
+            )
+        for offset in range(1, experts):
+            out_copy(slot, offset).start()
+        own_copy(slot).start()
+
+    @pl.when(layer < layers - 1)
+    def _():
+        row_copy(rows_ref, layer, 0).start()
+
+    @pl.when(layer > 0)
+    def _():
+        row_copy(rows_ref, layer, 1).start()
+
+    serve(layer, rows_ref)
+    for distance in range(1, layers):
+        for way in range(2):
+            slot = layer - distance if way == 0 else layer + distance
+            here = slot >= 0 if way == 0 else slot < layers
+            onward = layer < layers - 1 if way == 0 else layer > 0
+
+            @pl.when(here)
+            def _(slot=slot, way=way, onward=onward):
+                row_copy(rows_ref, slot, way).wait_recv()
+
+                @pl.when(onward)
+                def _():
+                    row_copy(held.at[slot], slot, way).start()
+
+                serve(slot, held.at[slot])
+
+    for slot in range(layers):
+
+        @pl.when((layer < layers - 1) & (slot <= layer))
+        def _(slot=slot):
+            row_copy(rows_ref, slot, 0).wait_send()
+
+        @pl.when((layer > 0) & (slot >= layer))
+        def _(slot=slot):
+            row_copy(rows_ref, slot, 1).wait_send()
+
+        for offset in range(1, experts):
+            out_copy(slot, offset).wait()
+        own_copy(slot).wait()
+
+
+def dispatch_rows(rows, picks, capacity):
+    count, cores = lax.axis_size("sp"), lax.axis_size("dp")
+    layers, across = plane_split(count)
+    experts = across * cores
+    tokens, features = rows.shape
+    vmem = pl.BlockSpec(memory_space=pltpu.VMEM)
+    return pl.pallas_call(
+        functools.partial(dispatch_kernel, layers, across, cores),
+        out_shape=jax.ShapeDtypeStruct((layers * experts, capacity, features), rows.dtype),
+        in_specs=[vmem, vmem],
+        out_specs=pl.BlockSpec(memory_space=pl.ANY),
+        scratch_shapes=[
+            pltpu.VMEM((layers, tokens, features), rows.dtype),
+            pltpu.VMEM((layers, experts, capacity, features), rows.dtype),
+            pltpu.SemaphoreType.DMA((2, layers)),
+            pltpu.SemaphoreType.DMA((layers,)),
+            pltpu.SemaphoreType.DMA((layers, experts)),
+            pltpu.SemaphoreType.DMA((layers, experts)),
+            pltpu.SemaphoreType.DMA((layers,)),
+        ],
+        compiler_params=pltpu.CompilerParams(collective_id=2, has_side_effects=True),
+    )(rows, picks)
+
+
+def combine_kernel(
+    layers, across, cores, rows_ref, high_ref, low_ref, out_ref, back, arrived, leaving,
+    back_send, back_recv, sum_send, sum_recv, local_sem,
+):
+    experts = across * cores
+    place = lax.axis_index("sp")
+    core = lax.axis_index("dp")
+    layer = lax.div(place, across)
+    column = lax.rem(place, across)
+    member = column * cores + core
+    capacity, features = back.shape[2:]
+    tile = features // 4
+
+    def peer_at(offset):
+        other = lax.rem(member + offset, experts)
+        where = {"sp": layer * across + lax.div(other, cores), "dp": lax.rem(other, cores)}
+        return other, where
+
+    def back_copy(slot, offset):
+        other, where = peer_at(offset)
+        return pltpu.make_async_remote_copy(
+            src_ref=rows_ref.at[slot * experts + other],
+            dst_ref=back.at[slot, member],
+            send_sem=back_send.at[slot, offset],
+            recv_sem=back_recv.at[slot, offset],
+            device_id=where,
+            device_id_type=MESH,
+        )
+
+    def own_copy(slot):
+        return pltpu.make_async_copy(
+            rows_ref.at[slot * experts + member], back.at[slot, member], local_sem.at[slot]
+        )
+
+    def sum_copy(slot, way):
+        step = 1 - 2 * way
+        return pltpu.make_async_remote_copy(
+            src_ref=leaving.at[slot],
+            dst_ref=arrived.at[way, slot],
+            send_sem=sum_send.at[slot],
+            recv_sem=sum_recv.at[way, slot],
+            device_id={"sp": lax.rem(place + step * across + layers * across, layers * across)},
+            device_id_type=MESH,
+        )
+
+    barrier = pltpu.get_barrier_semaphore()
+    for offset in range(1, experts):
+        pl.semaphore_signal(
+            barrier, inc=1, device_id=peer_at(offset)[1], device_id_type=MESH
+        )
+
+    @pl.when(layer > 0)
+    def _():
+        pl.semaphore_signal(
+            barrier, inc=1, device_id={"sp": place - across}, device_id_type=MESH
+        )
+
+    @pl.when(layer < layers - 1)
+    def _():
+        pl.semaphore_signal(
+            barrier, inc=1, device_id={"sp": place + across}, device_id_type=MESH
+        )
+
+    inner = (layer > 0) & (layer < layers - 1)
+
+    @pl.when(inner)
+    def _():
+        pl.semaphore_wait(barrier, experts + 1)
+
+    @pl.when(jnp.logical_not(inner))
+    def _():
+        pl.semaphore_wait(barrier, experts if layers > 1 else experts - 1)
+
+    def send_back(slot):
+        for offset in range(1, experts):
+            back_copy(slot, offset).start()
+        own_copy(slot).start()
+
+    def partial_sum(slot, columns):
+        produced = (
+            back[slot, :, :, columns]
+            .astype(jnp.float32)
+            .reshape(experts * capacity, tile)
+            .astype(jnp.bfloat16)
+        )
+        turned = (((0,), (0,)), ((), ()))
+        return lax.dot_general(
+            high_ref[slot], produced, turned, preferred_element_type=jnp.float32
+        ) + lax.dot_general(
+            low_ref[slot], produced, turned, preferred_element_type=jnp.float32
+        )
+
+    def gather_back(slot):
+        for offset in range(1, experts):
+            back_copy(slot, offset).wait()
+        own_copy(slot).wait()
+
+    for distance in range(layers - 1, 0, -1):
+        for way in range(2):
+            slot = layer + distance if way == 0 else layer - distance
+
+            @pl.when((slot < layers) if way == 0 else (slot >= 0))
+            def _(slot=slot):
+                send_back(slot)
+
+    send_back(layer)
+
+    for distance in range(layers - 1, 0, -1):
+        for way in range(2):
+            slot = layer + distance if way == 0 else layer - distance
+            upstream = layer > 0 if way == 0 else layer < layers - 1
+
+            @pl.when((slot < layers) if way == 0 else (slot >= 0))
+            def _(slot=slot, way=way, upstream=upstream):
+                gather_back(slot)
+
+                @pl.when(upstream)
+                def _():
+                    sum_copy(slot, way).wait_recv()
+                    for at in range(4):
+                        columns = slice(at * tile, (at + 1) * tile)
+                        leaving[slot, :, columns] = (
+                            partial_sum(slot, columns)
+                            + arrived[way, slot, :, columns].astype(jnp.float32)
+                        ).astype(jnp.bfloat16)
+
+                @pl.when(jnp.logical_not(upstream))
+                def _():
+                    for at in range(4):
+                        columns = slice(at * tile, (at + 1) * tile)
+                        leaving[slot, :, columns] = partial_sum(slot, columns).astype(
+                            jnp.bfloat16
+                        )
+
+                sum_copy(slot, way).start()
+
+    gather_back(layer)
+    for at in range(4):
+        columns = slice(at * tile, (at + 1) * tile)
+        out_ref[:, columns] = partial_sum(layer, columns)
+
+    for way in range(2):
+
+        @pl.when((layer > 0) if way == 0 else (layer < layers - 1))
+        def _(way=way):
+            sum_copy(layer, way).wait_recv()
+            out_ref[...] += arrived[way, layer].astype(jnp.float32)
+
+    for distance in range(1, layers):
+        for way in range(2):
+            slot = layer + distance if way == 0 else layer - distance
+
+            @pl.when((slot < layers) if way == 0 else (slot >= 0))
+            def _(slot=slot, way=way):
+                sum_copy(slot, way).wait_send()
+
+
+def combine_rows(produced, high, low):
+    count, cores = lax.axis_size("sp"), lax.axis_size("dp")
+    layers, across = plane_split(count)
+    experts = across * cores
+    capacity, features = produced.shape[1:]
+    tokens = high.shape[2]
+    vmem = pl.BlockSpec(memory_space=pltpu.VMEM)
+    return pl.pallas_call(
+        functools.partial(combine_kernel, layers, across, cores),
+        out_shape=jax.ShapeDtypeStruct((tokens, features), jnp.float32),
+        in_specs=[pl.BlockSpec(memory_space=pl.ANY), vmem, vmem],
+        out_specs=vmem,
+        scratch_shapes=[
+            pltpu.VMEM((layers, experts, capacity, features), produced.dtype),
+            pltpu.VMEM((2, layers, tokens, features), produced.dtype),
+            pltpu.VMEM((layers, tokens, features), produced.dtype),
+            pltpu.SemaphoreType.DMA((layers, experts)),
+            pltpu.SemaphoreType.DMA((layers, experts)),
+            pltpu.SemaphoreType.DMA((layers,)),
+            pltpu.SemaphoreType.DMA((2, layers)),
+            pltpu.SemaphoreType.DMA((layers,)),
+        ],
+        compiler_params=pltpu.CompilerParams(collective_id=3, has_side_effects=True),
+    )(produced, high, low)
+
+
+def plane_picks(ids, weights, capacity):
+    count, cores = lax.axis_size("sp"), lax.axis_size("dp")
+    layers, across = plane_split(count)
+    experts = across * cores
+    place = lax.axis_index("sp")
+    picks, tokens = ids.shape[1:]
+    ids = lax.dynamic_index_in_dim(
+        ids.reshape(layers, across, picks, tokens), lax.rem(place, across), 1, keepdims=False
+    )
+    mine = (lax.div(place, across) * experts + jnp.arange(experts)).astype(jnp.float32)
+    weights = lax.dynamic_index_in_dim(
+        weights.reshape(layers, across, picks, tokens), lax.rem(place, across), 1, keepdims=False
+    )
+    matches = ids[:, None] == mine[None, :, None, None]
+    named = jnp.any(matches, axis=2)
+    share = jnp.sum(jnp.where(matches, weights[:, None], 0.0), axis=2)[:, :, None, :]
+    order = jnp.arange(tokens)
+    before = (order[:, None] < order[None, :]).astype(jnp.bfloat16)
+    rank = jnp.dot(
+        named.astype(jnp.bfloat16).reshape(layers * experts, tokens),
+        before,
+        preferred_element_type=jnp.float32,
+    ).reshape(layers, experts, 1, tokens)
+    slots = jnp.arange(capacity, dtype=jnp.float32)[None, None, :, None]
+    chosen = named[:, :, None, :] & (rank == slots)
+    shape = (layers, experts * capacity, tokens)
+    share_high, share_low = halves(share)
+    none = jnp.zeros((), jnp.bfloat16)
+    return (
+        chosen.astype(jnp.bfloat16).reshape(shape),
+        jnp.where(chosen, share_high, none).reshape(shape),
+        jnp.where(chosen, share_low, none).reshape(shape),
+    )
+
+
 def layer_norm(values, gain):
     average = jnp.mean(values, -1, keepdims=True)
     centred = values - average
@@ -362,16 +735,30 @@
     tokens = query.shape[1]
     local_heads = head_decay_rate.shape[0]
     pieces = projection_pieces(output_projection)
+    picks = token_expert_index.shape[2]
+    spare = -(2 * local_heads + 2 * picks) % 8
     small = jnp.concatenate(
         [
-            write_strength_logit[0].T.reshape(count, local_heads, tokens),
-            decay_head_input[0].T.reshape(count, local_heads, tokens),
-            jnp.zeros((count, 8 - 2 * local_heads, tokens), jnp.bfloat16),
+            write_strength_logit[0].T.reshape(count, local_heads, tokens).astype(jnp.float32),
+            decay_head_input[0].T.reshape(count, local_heads, tokens).astype(jnp.float32),
+            jnp.broadcast_to(
+                token_expert_index[0].T.astype(jnp.float32)[None], (count, picks, tokens)
+            ),
+            jnp.broadcast_to(token_expert_weight[0].T[None], (count, picks, tokens)),
+            jnp.zeros((count, spare, tokens), jnp.float32),
         ],
         axis=1,
-    ).astype(jnp.float32)
+    )
     q_blocks, k_blocks, v_blocks, small_blocks = spread_heads(
         (query, key, value, small), count
+    )
+    experts = count * lax.axis_size("dp")
+    capacity = tokens * picks * 3 // (2 * experts)
+    first = 2 * local_heads
+    chosen, share_high, share_low = plane_picks(
+        small_blocks[:, first : first + picks],
+        small_blocks[:, first + picks : first + 2 * picks],
+        capacity,
     )
     added = added_log_decay[0].reshape(local_heads, count, tokens).transpose(1, 0, 2)
     scaled = recurrence(
@@ -392,42 +779,13 @@
     normed = layer_norm(residual[0].astype(jnp.float32) + mixed, mixer_norm_gain).astype(
         jnp.bfloat16
     )
-    experts = lax.axis_size("sp") * lax.axis_size("dp")
-    tok_rows = normed.shape[0]
-    picks = token_expert_index.shape[2]
-    features = normed.shape[1]
-    capacity = tok_rows * picks * 3 // (2 * experts)
-    flat_ids = token_expert_index[0].reshape(-1)
-    onehot = (flat_ids[:, None] == jnp.arange(experts, dtype=jnp.int32)[None, :]).astype(jnp.int32)
-    earlier = jnp.cumsum(onehot, axis=0) - onehot
-    slot_rank = jnp.sum(earlier * onehot, axis=1)
-    destination = flat_ids * capacity + slot_rank
-    source_token = (
-        jnp.full((experts * capacity,), tok_rows, jnp.int32)
-        .at[destination]
-        .set(jnp.arange(tok_rows * picks, dtype=jnp.int32) // picks)
-    )
-    padded = jnp.concatenate([normed, jnp.zeros((1, features), jnp.bfloat16)], 0)
-    dispatch = padded[source_token].reshape(experts, capacity, features)
-    back = lax.all_to_all(
-        expert_rows(
-            lax.all_to_all(dispatch, ("sp", "dp"), split_axis=0, concat_axis=0, tiled=True),
-            expert_gate_weight[0],
-            expert_up_weight[0],
-            expert_down_weight[0],
-        ),
-        ("sp", "dp"),
-        split_axis=0,
-        concat_axis=0,
-        tiled=True,
-    )
-    results = back.reshape(experts * capacity, features)[destination].reshape(
-        tok_rows, picks, features
-    )
-    weights = token_expert_weight[0]
-    moe = jnp.zeros((tok_rows, features), jnp.float32)
-    for pick in range(picks):
-        moe = moe + weights[:, pick : pick + 1] * results[:, pick].astype(jnp.float32)
+    produced = expert_rows(
+        dispatch_rows(normed, chosen, capacity),
+        expert_gate_weight[0],
+        expert_up_weight[0],
+        expert_down_weight[0],
+    )
+    moe = combine_rows(produced, share_high, share_low)
     return layer_norm(normed.astype(jnp.float32) + moe, feedforward_norm_gain)[None]
 
 

time: 278 us -> 224 us (0.81)
  Pallas kernels: 75.1 us -> 185 us
  blocking collectives: 78.6 us -> 0 us
  waiting for transfers between devices: 71.6 us -> 0.01 us
  local copies, waits for them, and re-layouts: 17.7 us -> 2.22 us
  starting transfers between devices: 6.73 us -> 3.07 us
  matrix products: 19 us -> 22.3 us
  other arithmetic: 7.91 us -> 11.1 us
    pallas_call x0 -> x2, Pallas kernels: none -> 109 us  [the longest x1 55.6 us: combine_rows(): pl.pallas_call(functools.partial(combine_kernel, layers, across, cores),...]
    all_to_all x1 -> x0, blocking collectives: 78.6 us -> none  [per_device(): lax.all_to_all(dispatch, ('sp', 'dp'), split_axis=0, concat_axis=0, tiled...]
    all_to_all x1 -> x0, waiting for transfers between devices: 71.6 us -> none  [per_device(): lax.all_to_all(expert_rows(lax.all_to_all(dispatch, ('sp', 'dp'), split_a...]
    gather x2 -> x0, local copies, waits for them, and re-layouts: 7.61 us -> none  [the longest x1 4.27 us: per_device(): dispatch = padded[source_token].reshape(experts, capacity, features)]
    all_to_all x1 -> x0, starting transfers between devices: 3.66 us -> none  [per_device(): lax.all_to_all(expert_rows(lax.all_to_all(dispatch, ('sp', 'dp'), split_a...]
    slice x2 -> x1, local copies, waits for them, and re-layouts: 3.29 us -> 0.01 us  [per_device(): small_blocks[:, first + picks:first + 2 * picks]]
    dot_general x1, matrix products: 3.45 us -> 6.57 us  [expert_rows(): jnp.dot(flat_rows, up_weight, preferred_element_type=jnp.float32)]
  transfers between devices with their start and end apart: 4 -> 3, of which waited for: 1 -> 0; matrix products, arithmetic and copies ran while one was open for 4% -> 5% of each run, Pallas kernels for 27% -> 34%
where the time goes in v1:
time: 224 us
  Pallas kernels  185 us (83%)
  matrix products  22.3 us (10%)
  other arithmetic  11.1 us (5%)
  starting transfers between devices  3.07 us (1%)
    pallas_call x1, Pallas kernels, combine_rows(): pl.pallas_call(functools.partial(combine_kernel, layers, across, cores),...  55.6 us
    pallas_call x1, Pallas kernels, dispatch_rows(): pl.pallas_call(functools.partial(dispatch_kernel, layers, across, cores),...  53.2 us
    pallas_call x1, Pallas kernels, spread_heads(): pl.pallas_call(functools.partial(spread_heads_kernel, count), out_shape=s...  33.2 us
    pallas_call x1, Pallas kernels, return_rows(): pl.pallas_call(functools.partial(return_rows_kernel, count), out_shape=ja...  24.2 us
    pallas_call x1, Pallas kernels, recurrence(): pl.pallas_call(recurrence_kernel, out_shape=jax.ShapeDtypeStruct(q_blocks...  18.4 us
    dot_general x4, matrix products, per_device(): jnp.dot(token_rows, piece, preferred_element_type=jnp.float32)  6.63 us
    dot_general x1, matrix products, expert_rows(): jnp.dot(flat_rows, up_weight, preferred_element_type=jnp.float32)  6.57 us
    dot_general x1, matrix products, expert_rows(): jnp.dot(hidden, down_weight, preferred_element_type=jnp.float32)  4.81 us
  transfers between devices with their start and end apart: 3, of which 0 were waited for; matrix products, arithmetic and copies ran while one was open for 5% of the time, Pallas kernels for 34%

profile of v1, /device:TPU:0, one launch (start us, length us, event | category | flops | bytes accessed | tf_op | source)
XLA Modules:
  0.0 223.6 jit_solution(8320192004688143757)
XLA Ops:
  0.5 2.5 %collective-permute-start.1 = (bf16[2048,512]{1,0:T(8,128)(2,1)}, bf16[2048,512]{1,0:T(8,128)(2,1)}, u32[]{:S(2)}, u32[]{:S(2)}) collective-permute-start(bf16[2048,512]{1,0:T(8,128)(2,1)} %param.28), channel_id=1, source_target_pairs={{0,2},{1,3},{2,0},{3,1},{4,6},{5,7},{6,4},{7,5},{8,10},{9,11},{10,... | collective-permute-start | bytes 6291464 | tf_op jit(solution)/shard_map/ppermute | solution.py:312
  3.0 0.7 convert_bitcast_fusion
  3.7 0.7 bitcast_convert_fusion.1
  4.4 0.7 bitcast_convert_fusion
  5.1 0.7 broadcast_in_dim.76
  5.8 1.3 concatenate.3.refs_3_
  7.0 33.2 %shard_map.172 = (bf16[8,128,256]{2,1,0:T(8,128)(2,1)}, bf16[8,128,256]{2,1,0:T(8,128)(2,1)}, bf16[8,128,256]{2,1,0:T(8,128)(2,1)}, f32[8,16,128]{2,1,0:T(8,128)}) custom-call(bf16[1,128,2048]{2,1,0:T(8,128)(2,1)} %refs_0_.1, bf16[1,128,2048]{2,1,0:T(8,128)(2,1)} %refs_1_.1, bf16[1,128,2048]{2,1,0:T(8,128)(2,1)} %refs_2_.1, f32[8,16,128]{2,1,0:T(8,128)} %concatenate.3.refs_3_), custom_call_target="tpu_custom_call" | custom-call | tf_op jit(solution)/shard_map/pallas_call | solution.py:76
  40.3 18.4 %shard_map.173.source = bf16[8,128,256]{2,1,0:T(8,128)(2,1)} custom-call(bf16[8,128,256]{2,1,0:T(8,128)(2,1)} %get-tuple-element.9.q_ref, bf16[8,128,256]{2,1,0:T(8,128)(2,1)} %get-tuple-element.10.k_ref, bf16[8,128,256]{2,1,0:T(8,128)(2,1)} %get-tuple-element.11.v_ref, f32[8,16,128]{2,1,0:T(8,128)} %get-tuple-element.12.small_ref, f32[8,2,128]{2,1,0:T(2,128)} %bitcast.103, ...), custom_call_target="tpu_custom_call" | custom-call | flops 42949672960 | bytes 2097152 | tf_op jit(solution)/shard_map/pallas_call | solution.py:282
  58.8 24.2 %shard_map.174 = bf16[128,2048]{1,0:T(8,128)(2,1)} custom-call(bf16[8,128,256]{2,1,0:T(8,128)(2,1)} %shard_map.173.source), custom_call_target="tpu_custom_call" | custom-call | tf_op jit(solution)/shard_map/pallas_call | solution.py:116
  83.4 0.8 fusion.21.pick_ref
  84.3 0.9 fusion.19
  85.2 1.4 fusion.15
  87.2 2.0 convolution_dynamic-update-slice_fusion.2
  89.2 2.1 convolution_dynamic-update-slice_fusion.1
  91.3 2.0 convolution_dynamic-update-slice_fusion
  93.9 1.0 multiply_convert_fusion.1.rows_ref
  94.9 53.2 %shard_map.175 = bf16[32,24,2048]{2,1,0:T(8,128)(2,1)} custom-call(bf16[128,2048]{1,0:T(8,128)(2,1)} %multiply_convert_fusion.1.rows_ref, bf16[4,192,128]{2,1,0:T(8,128)(2,1)} %fusion.21.pick_ref), custom_call_target="tpu_custom_call" | custom-call | tf_op jit(solution)/shard_map/pallas_call | solution.py:458
  148.1 6.6 %fusion.2 = f32[768,1024]{1,0:T(8,128)S(1)} fusion(bf16[768,2048]{1,0:T(8,128)(2,1)} %bitcast.96, bf16[1,2048,1024]{2,1,0:T(8,128)(2,1)} %param.33), kind=kOutput, calls=%fused_computation.2 | convolution fusion | flops 3221225472 | bytes 10485760 | tf_op jit(solution)/shard_map/dot_general | solution.py:707
  154.7 4.1 %multiply_convert_fusion = bf16[768,1024]{1,0:T(8,128)(2,1)S(1)} fusion(f32[768,1024]{1,0:T(8,128)S(1)} %fusion.2, bf16[768,2048]{1,0:T(8,128)(2,1)S(1)} %bitcast.97, bf16[1,2048,1024]{2,1,0:T(8,128)(2,1)S(1)} %copy-done.9), kind=kOutput, calls=%fused_computation.7 | convolution fusion | flops 3229089792 | bytes 12058624 | tf_op jit(solution)/shard_map/dot_general | solution.py:704
  158.9 4.8 %fusion.6 = bf16[768,2048]{1,0:T(8,128)(2,1)} fusion(bf16[768,1024]{1,0:T(8,128)(2,1)S(1)} %multiply_convert_fusion, bf16[1,1024,2048]{2,1,0:T(8,128)(2,1)S(1)} %copy-done.10), kind=kOutput, calls=%fused_computation.6 | convolution fusion | flops 3222798336 | bytes 8912896 | tf_op jit(solution)/shard_map/dot_general | solution.py:710
  163.7 55.6 %shard_map.176 = f32[128,2048]{1,0:T(8,128)} custom-call(bf16[32,24,2048]{2,1,0:T(8,128)(2,1)} %bitcast.95, bf16[4,192,128]{2,1,0:T(8,128)(2,1)} %get-tuple-element.18.high_ref, bf16[4,192,128]{2,1,0:T(8,128)(2,1)} %get-tuple-element.17.low_ref), custom_call_target="tpu_custom_call" | custom-call | tf_op jit(solution)/shard_map/pallas_call | solution.py:640
  219.3 1.5 fusion.16
  220.8 1.5 multiply_reduce_fusion
  222.4 1.2 multiply_bitcast_fusion
  (46 shorter events, 2.1 us)
Async XLA Ops:
  0.0 87.1 %collective-permute-start = (bf16[2048,512]{1,0:T(8,128)(2,1)}, bf16[2048,512]{1,0:T(8,128)(2,1)}, u32[]{:S(2)}, u32[]{:S(2)}) collective-permute-start(bf16[2048,512]{1,0:T(8,128)(2,1)} %param.28), channel_id=1, source_target_pairs={{0,1},{1,0},{2,3},{3,2},{4,5},{5,4},{6,7},{7,6},{8,9},{9,8},{10,11... | collective-permute-start | bytes 6291464 | tf_op jit(solution)/shard_map/ppermute | solution.py:317
  0.5 58.2 %collective-permute-start.1 = (bf16[2048,512]{1,0:T(8,128)(2,1)}, bf16[2048,512]{1,0:T(8,128)(2,1)}, u32[]{:S(2)}, u32[]{:S(2)}) collective-permute-start(bf16[2048,512]{1,0:T(8,128)(2,1)} %param.28), channel_id=1, source_target_pairs={{0,2},{1,3},{2,0},{3,1},{4,6},{5,7},{6,4},{7,5},{8,10},{9,11},{10,... | collective-permute-start | bytes 6291464 | tf_op jit(solution)/shard_map/ppermute | solution.py:312
  40.3 18.4 %copy-start.6 = (f32[8,16,128]{2,1,0:T(8,128)S(1)}, f32[8,16,128]{2,1,0:T(8,128)}, u32[]{:S(2)}) copy-start(f32[8,16,128]{2,1,0:T(8,128)} %get-tuple-element.12.small_ref) | copy-start | bytes 196612
  40.3 44.9 %copy-start.5 = (bf16[1,128,2048]{2,1,0:T(8,128)(2,1)S(1)}, bf16[1,128,2048]{2,1,0:T(8,128)(2,1)}, u32[]{:S(2)}) copy-start(bf16[1,128,2048]{2,1,0:T(8,128)(2,1)} %param.22) | copy-start | bytes 1572868
  58.7 28.0 %copy-start.4 = (bf16[2048,512]{1,0:T(8,128)(2,1)S(1)}, bf16[2048,512]{1,0:T(8,128)(2,1)}, u32[]{:S(2)}) copy-start(bf16[2048,512]{1,0:T(8,128)(2,1)} %param.28) | copy-start | bytes 6291460
  58.7 32.6 %collective-permute-start.2 = (bf16[2048,512]{1,0:T(8,128)(2,1)}, bf16[2048,512]{1,0:T(8,128)(2,1)}, u32[]{:S(2)}, u32[]{:S(2)}) collective-permute-start(bf16[2048,512]{1,0:T(8,128)(2,1)} %collective-permute-done.1), channel_id=1, source_target_pairs={{0,1},{1,0},{2,3},{3,2},{4,5},{5,4},{6,7},{7,6},{8,9},{9,8},{10,11... | collective-permute-start | bytes 6291464 | tf_op jit(solution)/shard_map/ppermute | solution.py:317
  89.2 4.2 %copy-start.2 = (bf16[1,128,2048]{2,1,0:T(8,128)(2,1)S(1)}, bf16[1,128,2048]{2,1,0:T(8,128)(2,1)}, u32[]{:S(2)}) copy-start(bf16[1,128,2048]{2,1,0:T(8,128)(2,1)} %param.18) | copy-start | bytes 1572868
  91.3 2.6 %copy-start.7 = (f32[2048]{0:T(1024)S(1)}, f32[2048]{0:T(1024)}, u32[]{:S(2)}) copy-start(f32[2048]{0:T(1024)} %param.29) | copy-start | bytes 24580
  148.1 6.6 %copy-start.3 = (bf16[32,24,2048]{2,1,0:T(8,128)(2,1)S(1)}, bf16[32,24,2048]{2,1,0:T(8,128)(2,1)}, u32[]{:S(2)}) copy-start(bf16[32,24,2048]{2,1,0:T(8,128)(2,1)} %shard_map.175) | copy-start | bytes 9437188
  148.1 6.6 %copy-start.9 = (bf16[1,2048,1024]{2,1,0:T(8,128)(2,1)S(1)}, bf16[1,2048,1024]{2,1,0:T(8,128)(2,1)}, u32[]{:S(2)}) copy-start(bf16[1,2048,1024]{2,1,0:T(8,128)(2,1)} %param.32) | copy-start | bytes 12582916
  154.7 4.2 %copy-start.10 = (bf16[1,1024,2048]{2,1,0:T(8,128)(2,1)S(1)}, bf16[1,1024,2048]{2,1,0:T(8,128)(2,1)}, u32[]{:S(2)}) copy-start(bf16[1,1024,2048]{2,1,0:T(8,128)(2,1)} %param.34) | copy-start | bytes 12582916
  163.7 55.6 %copy-start.1 = (bf16[128,2048]{1,0:T(8,128)(2,1)S(1)}, bf16[128,2048]{1,0:T(8,128)(2,1)}, u32[]{:S(2)}) copy-start(bf16[128,2048]{1,0:T(8,128)(2,1)} %multiply_convert_fusion.1.rows_ref) | copy-start | bytes 1572868
  163.7 58.7 %copy-start.8 = (f32[2048]{0:T(1024)S(1)}, f32[2048]{0:T(1024)}, u32[]{:S(2)}) copy-start(f32[2048]{0:T(1024)} %param.35) | copy-start | bytes 24580
  219.3 3.0 %copy-start = (f32[128,2048]{1,0:T(8,128)S(1)}, f32[128,2048]{1,0:T(8,128)}, u32[]{:S(2)}) copy-start(f32[128,2048]{1,0:T(8,128)} %shard_map.176) | copy-start | bytes 3145732
